TPU v7x, 256 devices: a whole 4x4x8 slice. The times are simulated.
256 devices in a mesh: fs: 32 (over z, x), tp: 8 (over y, core).
Axes of the slice: x: 4, y: 4, z: 8, core: 2. Of those that a mesh axis runs over, the one named last changes fastest.
Arguments:
- tokens: bfloat16 [16384, 2048], P('fs', 'tp'), may hold values from -16 to 16
- pre_mix_gain: bfloat16 [2048], P('tp'), may hold values from 0.099609375 to 1.8984375
- w_gate_in: bfloat16 [2048, 2048], P('fs', 'tp'), may hold values from -0.125 to 0.125
- w_input: bfloat16 [2048, 2048], P('fs', 'tp'), may hold values from -0.125 to 0.125
- mix_kernel: bfloat16 [4, 2048], P(None, 'tp'), may hold values from -3 to 3
- w_recur: bfloat16 [8, 256, 256], P('tp'), may hold values from -0.375 to 0.375
- w_inject: bfloat16 [8, 256, 256], P('tp'), may hold values from -0.375 to 0.375
- decay_param: float32 [2048], P('tp'), may hold values from 3 to 13
- w_mix_out: bfloat16 [2048, 2048], P('tp', 'fs'), may hold values from -0.125 to 0.125
- post_mix_gain: bfloat16 [2048], P('tp'), may hold values from 0.099609375 to 1.8984375
- pre_ffn_gain: bfloat16 [2048], P('tp'), may hold values from 0.099609375 to 1.8984375
- w_up_gate: bfloat16 [2048, 5632], P('fs', 'tp'), may hold values from -0.125 to 0.125
- w_up_value: bfloat16 [2048, 5632], P('fs', 'tp'), may hold values from -0.125 to 0.125
- gate_kernel: bfloat16 [3, 5632], P(None, 'tp'), may hold values from -3 to 3
- value_kernel: bfloat16 [3, 5632], P(None, 'tp'), may hold values from -3 to 3
- w_down: bfloat16 [5632, 2048], P('tp', 'fs'), may hold values from -0.078125 to 0.078125
- post_ffn_gain: bfloat16 [2048], P('tp'), may hold values from 0.099609375 to 1.8984375
Outputs:
- layer_out: bfloat16 [16384, 2048], P('fs', 'tp')
All inputs are finite; a program needn't handle non-finite values.
Results may differ from a plain program's by a relative error of at most 0.015.
Values may be sent and summed in bfloat16 or wider, within the bound.
No kernel may reach another device: no remote copies, remote signals or barrier semaphores. Data moves between devices by JAX's collectives and lax.ppermute only.
A program may use at most 64 MiB of HBM per device.

v0:
```python
import jax
import jax.numpy as jnp
from jax import lax
from jax.sharding import Mesh
from jax.sharding import PartitionSpec as P

D = 2048
FS = ("fs_0", "fs_1")


norm_eps = 1e-06
gate_power = 8.0


def sent_to_all(shard, axis):
    devices = lax.axis_size(axis)
    return lax.all_to_all(
        jnp.broadcast_to(shard[None], (devices, *shard.shape)), axis, 0, 0, tiled=True
    )


def taken_together(shard, axis):
    return sent_to_all(shard, axis).sum(axis=0)


def laid_out(pieces, dim):
    pieces = jnp.moveaxis(pieces, 0, dim)
    shape = pieces.shape
    return pieces.reshape(*shape[:dim], shape[dim] * shape[dim + 1], *shape[dim + 2 :])


def gather_directly(shard, axis, dim):
    return laid_out(sent_to_all(shard, axis), dim)


def split_up(shard, dim, devices):
    shape = shard.shape
    pieces = shard.reshape(*shape[:dim], devices, shape[dim] // devices, *shape[dim + 1 :])
    return jnp.moveaxis(pieces, dim, 0)


def sent_and_summed(shard, axis, dim):
    devices = lax.axis_size(axis)
    pieces = lax.all_to_all(split_up(shard, dim, devices), axis, 0, 0, tiled=True)
    return jnp.sum(pieces.astype(jnp.float32), axis=0)


def gather_turned(arrays, axis, dims):
    turned = [jnp.moveaxis(a, dim, 0) for a, dim in zip(arrays, dims)]
    widths = [t[0].size for t in turned]
    both = jnp.concatenate([t.reshape(-1, w) for t, w in zip(turned, widths)], axis=1)
    filled = lax.all_gather(both, axis, axis=0, tiled=True)
    pieces = jnp.split(filled, [sum(widths[:k]) for k in range(1, len(widths))], axis=1)
    return tuple(
        (
            jnp.moveaxis(b.reshape(-1, *t.shape[1:]), 0, dim)
            for b, t, dim in zip(pieces, turned, dims)
        )
    )


def in_one_piece(arrays, axis, dim, along):
    ends, at = ([], 0)
    for a in arrays[:-1]:
        at += a.shape[along]
        ends.append(at)
    both = jnp.concatenate(arrays, axis=along)
    return tuple(jnp.split(lax.all_gather(both, axis, axis=dim, tiled=True), ends, axis=along))


def gather_axes(shard, axes, dim):
    for axis in reversed(axes):
        shard = lax.all_gather(shard, axis, axis=dim, tiled=True)
    return shard


def row_normed(values, row_gain):
    widened = values.astype(jnp.float32)
    squares = taken_together(jnp.sum(widened * widened, axis=1), "tp")
    factor = lax.rsqrt(squares / D + norm_eps)
    return widened * factor[:, None] * row_gain.astype(jnp.float32)[None, :]


def gathered_rows(values, row_gain):
    return gather_directly(row_normed(values, row_gain).astype(jnp.bfloat16), "tp", 1)


def summed_terms(partial_value):
    return sent_and_summed(partial_value.astype(jnp.bfloat16), "tp", 1)


def causal_conv(values, kernel):
    length = values.shape[0]
    widths = kernel.shape[0]
    padded = jnp.pad(values.astype(jnp.float32), ((widths - 1, 0), (0, 0)))
    weights = kernel.astype(jnp.float32)
    result = padded[0:length] * weights[0]
    for offset in range(1, widths):
        result = result + padded[offset : offset + length] * weights[offset]
    return result


def pair_folder(inputs, pieces):
    return (
        jnp.dot(inputs, pieces[0], preferred_element_type=jnp.float32),
        jnp.dot(inputs, pieces[1], preferred_element_type=jnp.float32),
    )


def linear_combine(earlier, latter):
    return (earlier[0] * latter[0], latter[0] * earlier[1] + latter[1])


def shards(
    tokens,
    pre_mix_gain,
    w_gate_in,
    w_input,
    mix_kernel,
    w_recur,
    w_inject,
    decay_param,
    w_mix_out,
    post_mix_gain,
    pre_ffn_gain,
    w_up_gate,
    w_up_value,
    gate_kernel,
    value_kernel,
    w_down,
    post_ffn_gain,
):
    whole_gate, whole_value, whole_down = gather_turned(
        (w_up_gate, w_up_value, w_down), FS, (0, 0, 1)
    )
    normed_in = gathered_rows(tokens, pre_mix_gain)
    length = normed_in.shape[0]
    gate_sum, input_sum = pair_folder(normed_in, in_one_piece((w_gate_in, w_input), FS, 0, 1))
    gate_rows = gate_sum.astype(jnp.bfloat16)
    input_rows = input_sum.astype(jnp.bfloat16)
    smoothed = causal_conv(input_rows, mix_kernel).astype(jnp.bfloat16)
    by_head = smoothed.reshape(length, w_recur.shape[0], w_recur.shape[1])
    recur_gate = jax.nn.sigmoid(
        jnp.einsum("thi,hij->thj", by_head, w_recur, preferred_element_type=jnp.float32)
    ).reshape(length, -1)
    inject_gate = jax.nn.sigmoid(
        jnp.einsum("thi,hij->thj", by_head, w_inject, preferred_element_type=jnp.float32)
    ).reshape(length, -1)
    log_retain = -gate_power * recur_gate * jax.nn.softplus(-decay_param)[None, :]
    retain = jnp.exp(log_retain)
    driven = jnp.sqrt(-jnp.expm1(2.0 * log_retain)) * inject_gate * smoothed.astype(jnp.float32)
    _, states = lax.associative_scan(linear_combine, (retain, driven), axis=0)
    hidden = (jax.nn.gelu(gate_rows.astype(jnp.float32), approximate=True) * states).astype(
        jnp.bfloat16
    )
    mixer_terms = jnp.dot(hidden, gather_axes(w_mix_out, FS, 1), preferred_element_type=jnp.float32)
    middle = (
        tokens.astype(jnp.float32) + row_normed(summed_terms(mixer_terms), post_mix_gain)
    ).astype(jnp.bfloat16)
    normed_mid = gathered_rows(middle, pre_ffn_gain)
    up_gate = jnp.dot(normed_mid, whole_gate, preferred_element_type=jnp.float32)
    up_value = jnp.dot(normed_mid, whole_value, preferred_element_type=jnp.float32)
    conv_gate_out = causal_conv(up_gate.astype(jnp.bfloat16), gate_kernel)
    conv_value_out = causal_conv(up_value.astype(jnp.bfloat16), value_kernel)
    activated = (jax.nn.gelu(conv_gate_out, approximate=True) * conv_value_out).astype(jnp.bfloat16)
    ffn_terms = jnp.dot(activated, whole_down, preferred_element_type=jnp.float32)
    return (middle.astype(jnp.float32) + row_normed(summed_terms(ffn_terms), post_ffn_gain)).astype(
        jnp.bfloat16
    )


def solution(mesh):
    finer = Mesh(mesh.devices.reshape(8, 4, mesh.shape["tp"]), ("fs_0", "fs_1", "tp"))
    return jax.shard_map(
        shards,
        mesh=finer,
        in_specs=(
            P(FS, "tp"),
            P("tp"),
            P(FS, "tp"),
            P(FS, "tp"),
            P(None, "tp"),
            P("tp", None, None),
            P("tp", None, None),
            P("tp"),
            P("tp", FS),
            P("tp"),
            P("tp"),
            P(FS, "tp"),
            P(FS, "tp"),
            P(None, "tp"),
            P(None, "tp"),
            P("tp", FS),
            P("tp"),
        ),
        out_specs=P(FS, "tp"),
        check_vma=False,
    )
```

profile of v0, /device:TPU:1, one launch (start us, length us, event | category | flops | bytes accessed | tf_op | source)
XLA Modules:
  0.0 321.6 jit_solution(9744152567858369180)
XLA Ops:
  8.1 12.0 %all_gather.13 = bf16[256,256]{0,1:T(8,128)(2,1)} all-gather(bf16[256,64]{0,1:T(8,128)(2,1)} %param.25), channel_id=1, replica_groups=mesh['fs_0'=8,'fs_1'=4,'tp'=8] {'fs_1'}, dimensions={1}, use_global_device_ids=true | all-gather | bytes 163840 | tf_op jit(solution)/shard_map/all_gather | solution.py:73
  20.2 1.8 concatenate.39
  23.8 7.8 %all-to-all-start = ((f32[8,1,512]{2,1,0:T(1,128)}), f32[8,1,512]{2,1,0:T(1,128)S(1)}, u32[]{:S(2)}, u32[]{:S(2)}) async-start(f32[8,1,512]{2,1,0:T(1,128)} %broadcast_in_dim.12), calls=%async_computation | async-start | bytes 32768 | tf_op jit(solution)/shard_map/all_to_all | solution.py:17
  32.2 4.1 %all-to-all-done = f32[8,1,512]{2,1,0:T(1,128)S(1)} async-done(((f32[8,1,512]{2,1,0:T(1,128)}), f32[8,1,512]{2,1,0:T(1,128)S(1)}, u32[]{:S(2)}, u32[]{:S(2)}) %all-to-all-start) | async-done | bytes 16416 | tf_op jit(solution)/shard_map/all_to_all | solution.py:17
  37.5 1.5 broadcast_in_dim.13
  39.1 4.3 %all-to-all-start.1 = ((bf16[8,512,256]{1,2,0:T(8,128)(2,1)}), bf16[8,512,256]{1,2,0:T(8,128)(2,1)S(1)}, u32[]{:S(2)}, u32[]{:S(2)}) async-start(bf16[8,512,256]{1,2,0:T(8,128)(2,1)} %broadcast_in_dim.13), calls=%async_computation.1 | async-start | bytes 4194304 | tf_op jit(solution)/shard_map/all_to_all | solution.py:17
  43.4 26.2 %all-to-all-done.1 = bf16[8,512,256]{1,2,0:T(8,128)(2,1)S(1)} async-done(((bf16[8,512,256]{1,2,0:T(8,128)(2,1)}), bf16[8,512,256]{1,2,0:T(8,128)(2,1)S(1)}, u32[]{:S(2)}, u32[]{:S(2)}) %all-to-all-start.1) | async-done | bytes 2097184 | tf_op jit(solution)/shard_map/all_to_all | solution.py:17
  69.6 17.5 %all-gather.4.cloned.1.call-done = bf16[2048,512]{1,0:T(8,128)(2,1)} async-done(((bf16[64,512]{1,0:T(8,128)(2,1)}), bf16[2048,512]{1,0:T(8,128)(2,1)}) %all-gather.4.cloned.1.call-update) | async-done | bytes 2097168 | tf_op jit(solution)/shard_map/all_gather | solution.py:68
  87.0 2.0 fusion.48
  102.6 1.6 fusion.118
  104.1 1.4 slice.289
  108.5 1.5 slice.292
  144.6 1.5 slice.287
  146.1 1.4 slice.328
  153.1 2.5 slice.269
  165.3 2.6 pad.84
  168.1 5.5 %convolution_convert_fusion = bf16[512,2048]{1,0:T(8,128)(2,1)} fusion(bf16[256,2048]{0,1:T(8,128)(2,1)} %all-gather.6.cloned.1.call-done, bf16[512,2048]{0,1:T(8,128)(2,1)S(1)} %bitcast.43, bf16[2048,512]{1,0:T(8,128)(2,1)} %all-gather.4.cloned.1.call-done, f32[512,256]{1,0:T(8,128)S(1)} %pad.83, f32[512,256]{1,0:T(8,128)} %pad.84), kind=kOutput, calls=%fused_computation.8 | convolution fusion | flops 1076494336 | bytes 7340032 | tf_op jit(solution)/shard_map/dot_general | solution.py:156
  173.6 1.7 copy.45
  175.3 35.6 %all_to_all.44 = bf16[8,512,256]{2,1,0:T(8,128)(2,1)S(1)} all-to-all(bf16[8,512,256]{2,1,0:T(8,128)(2,1)S(1)} %bitcast.40), channel_id=1, replica_groups=mesh['fs_0'=8,'fs_1'=4,'tp'=8] {'tp'}, dimensions={0} | all-to-all | bytes 4194304 | tf_op jit(solution)/shard_map/all_to_all | solution.py:44
  212.0 4.2 %all-to-all-start.3 = ((f32[8,1,512]{2,1,0:T(1,128)}), f32[8,1,512]{2,1,0:T(1,128)S(1)}, u32[]{:S(2)}, u32[]{:S(2)}) async-start(f32[8,1,512]{2,1,0:T(1,128)} %broadcast_in_dim.14), calls=%async_computation.3 | async-start | bytes 32768 | tf_op jit(solution)/shard_map/all_to_all | solution.py:17
  216.2 4.7 %all-to-all-done.3 = f32[8,1,512]{2,1,0:T(1,128)S(1)} async-done(((f32[8,1,512]{2,1,0:T(1,128)}), f32[8,1,512]{2,1,0:T(1,128)S(1)}, u32[]{:S(2)}, u32[]{:S(2)}) %all-to-all-start.3) | async-done | bytes 16416 | tf_op jit(solution)/shard_map/all_to_all | solution.py:17
  221.9 3.9 %all-to-all-start.4 = ((f32[8,1,512]{2,1,0:T(1,128)}), f32[8,1,512]{2,1,0:T(1,128)S(1)}, u32[]{:S(2)}, u32[]{:S(2)}) async-start(f32[8,1,512]{2,1,0:T(1,128)} %broadcast_in_dim.15), calls=%async_computation.4 | async-start | bytes 32768 | tf_op jit(solution)/shard_map/all_to_all | solution.py:17
  225.8 4.7 %all-to-all-done.4 = f32[8,1,512]{2,1,0:T(1,128)S(1)} async-done(((f32[8,1,512]{2,1,0:T(1,128)}), f32[8,1,512]{2,1,0:T(1,128)S(1)}, u32[]{:S(2)}, u32[]{:S(2)}) %all-to-all-start.4) | async-done | bytes 16416 | tf_op jit(solution)/shard_map/all_to_all | solution.py:17
  230.8 1.6 broadcast_in_dim.16
  232.3 4.3 %all-to-all-start.5 = ((bf16[8,512,256]{1,2,0:T(8,128)(2,1)}), bf16[8,512,256]{1,2,0:T(8,128)(2,1)S(1)}, u32[]{:S(2)}, u32[]{:S(2)}) async-start(bf16[8,512,256]{1,2,0:T(8,128)(2,1)} %broadcast_in_dim.16), calls=%async_computation.5 | async-start | bytes 4194304 | tf_op jit(solution)/shard_map/all_to_all | solution.py:17
  236.8 26.1 %all-to-all-done.5 = bf16[8,512,256]{1,2,0:T(8,128)(2,1)S(1)} async-done(((bf16[8,512,256]{1,2,0:T(8,128)(2,1)}), bf16[8,512,256]{1,2,0:T(8,128)(2,1)S(1)}, u32[]{:S(2)}, u32[]{:S(2)}) %all-to-all-start.5) | async-done | bytes 2097184 | tf_op jit(solution)/shard_map/all_to_all | solution.py:17
  262.9 3.7 %fusion.29 = f32[512,704]{0,1:T(8,128)S(1)} fusion(bf16[512,2048]{0,1:T(8,128)(2,1)S(1)} %bitcast.44, bf16[2048,2112]{1,0:T(8,128)(2,1)} %all-gather.8.cloned.1.call-done), kind=kOutput, calls=%fused_computation.35 | convolution fusion | flops 1477115904 | bytes 6684672 | tf_op jit(solution)/shard_map/dot_general | solution.py:161
  267.4 2.9 fusion.35
  270.3 4.1 %fusion.6 = bf16[512,2048]{1,0:T(8,128)(2,1)S(1)} fusion(bf16[2048,2112]{1,0:T(8,128)(2,1)S(1)} %copy-done.14, f32[512,704]{0,1:T(8,128)S(1)} %fusion.35, f32[512,704]{0,1:T(8,128)S(1)} %fusion.29, f32[704]{0:T(1024)S(1)} %get-tuple-element.9, f32[704]{0:T(1024)S(1)} %get-tuple-element.10, f32[704]{0:T(1024)S(1)} %get-tuple-element.8, ...), kind=kOutput, calls=%fused_computation.9 | convolution fusion | flops 1484652544 | bytes 8151040 | tf_op jit(solution)/shard_map/dot_general | solution.py:166
  274.5 29.6 %all_to_all.45 = bf16[8,512,256]{2,1,0:T(8,128)(2,1)S(1)} all-to-all(bf16[8,512,256]{2,1,0:T(8,128)(2,1)S(1)} %bitcast.41), channel_id=1, replica_groups=mesh['fs_0'=8,'fs_1'=4,'tp'=8] {'tp'}, dimensions={0} | all-to-all | bytes 4194304 | tf_op jit(solution)/shard_map/all_to_all | solution.py:44
  305.2 4.3 %all-to-all-start.7 = ((f32[8,1,512]{2,1,0:T(1,128)}), f32[8,1,512]{2,1,0:T(1,128)S(1)}, u32[]{:S(2)}, u32[]{:S(2)}) async-start(f32[8,1,512]{2,1,0:T(1,128)} %broadcast_in_dim.17), calls=%async_computation.7 | async-start | bytes 32768 | tf_op jit(solution)/shard_map/all_to_all | solution.py:17
  309.5 4.7 %all-to-all-done.7 = f32[8,1,512]{2,1,0:T(1,128)S(1)} async-done(((f32[8,1,512]{2,1,0:T(1,128)}), f32[8,1,512]{2,1,0:T(1,128)S(1)}, u32[]{:S(2)}, u32[]{:S(2)}) %all-to-all-start.7) | async-done | bytes 16416 | tf_op jit(solution)/shard_map/all_to_all | solution.py:17
  (179 shorter events, 76.8 us)
Async XLA Ops:
  6.5 82.7 %copy-start = (bf16[1,256,256]{2,1,0:T(8,128)(2,1)S(1)}, bf16[1,256,256]{2,1,0:T(8,128)(2,1)}, u32[]{:S(2)}) copy-start(bf16[1,256,256]{2,1,0:T(8,128)(2,1)} %param.22) | copy-start | bytes 393220
  6.5 80.5 %all-gather.4.cloned.1.call-start = ((), (), s32[]{:S(2)}) async-start(), calls=%async_computation.8 | async-start | bytes 2162688 | tf_op jit(solution)/shard_map/all_gather | solution.py:68
  8.0 160.1 %all-gather.6.cloned.1.call-start = ((), (), s32[]{:S(2)}) async-start(), calls=%async_computation.9 | async-start | bytes 1179648 | tf_op jit(solution)/shard_map/all_gather | solution.py:73
  20.1 242.8 %all-gather.8.cloned.1.call-start = ((), (), s32[]{:S(2)}) async-start(), calls=%async_computation.10 | async-start | bytes 9191424 | tf_op jit(solution)/shard_map/all_gather | solution.py:52
  23.8 12.5 %all-to-all-start = ((f32[8,1,512]{2,1,0:T(1,128)}), f32[8,1,512]{2,1,0:T(1,128)S(1)}, u32[]{:S(2)}, u32[]{:S(2)}) async-start(f32[8,1,512]{2,1,0:T(1,128)} %broadcast_in_dim.12), calls=%async_computation | async-start | bytes 32768 | tf_op jit(solution)/shard_map/all_to_all | solution.py:17
  39.1 4.3 %copy-start.13 = (f32[256]{0:T(256)S(1)}, f32[256]{0:T(256)}, u32[]{:S(2)}) copy-start(f32[256]{0:T(256)} %param.24) | copy-start | bytes 3076
  39.1 4.3 %copy-start.9 = (bf16[4,256]{1,0:T(4,128)(2,1)S(1)}, bf16[4,256]{1,0:T(4,128)(2,1)}, u32[]{:S(2)}) copy-start(bf16[4,256]{1,0:T(4,128)(2,1)} %param.21) | copy-start | bytes 6148
  39.1 30.5 %all-to-all-start.1 = ((bf16[8,512,256]{1,2,0:T(8,128)(2,1)}), bf16[8,512,256]{1,2,0:T(8,128)(2,1)S(1)}, u32[]{:S(2)}, u32[]{:S(2)}) async-start(bf16[8,512,256]{1,2,0:T(8,128)(2,1)} %broadcast_in_dim.13), calls=%async_computation.1 | async-start | bytes 4194304 | tf_op jit(solution)/shard_map/all_to_all | solution.py:17
  89.0 0.9 copy-start.15
  89.6 3.9 %copy-start.3 = (f32[512,256]{1,0:T(8,128)}, f32[512,256]{1,0:T(8,128)S(1)}, u32[]{:S(2)}) copy-start(f32[512,256]{1,0:T(8,128)S(1)} %get-tuple-element.35) | copy-start | bytes 1572868
  90.4 65.2 %copy-start.2 = (f32[512,256]{1,0:T(8,128)}, f32[512,256]{1,0:T(8,128)S(1)}, u32[]{:S(2)}) copy-start(f32[512,256]{1,0:T(8,128)S(1)} %fusion.46) | copy-start | bytes 1572868
  152.2 12.2 %copy-start.5 = (f32[127,256]{1,0:T(8,128)S(1)}, f32[127,256]{1,0:T(8,128)}, u32[]{:S(2)}) copy-start(f32[127,256]{1,0:T(8,128)} %slice.332) | copy-start | bytes 390148
  152.2 12.2 %copy-start.6 = (f32[127,256]{1,0:T(8,128)S(1)}, f32[127,256]{1,0:T(8,128)}, u32[]{:S(2)}) copy-start(f32[127,256]{1,0:T(8,128)} %slice.275) | copy-start | bytes 390148
  152.8 10.8 %copy-start.7 = (f32[63,256]{1,0:T(8,128)S(1)}, f32[63,256]{1,0:T(8,128)}, u32[]{:S(2)}) copy-start(f32[63,256]{1,0:T(8,128)} %slice.281) | copy-start | bytes 193540
  152.8 10.9 %copy-start.8 = (f32[63,256]{1,0:T(8,128)S(1)}, f32[63,256]{1,0:T(8,128)}, u32[]{:S(2)}) copy-start(f32[63,256]{1,0:T(8,128)} %slice.330) | copy-start | bytes 193540
  155.6 8.8 %copy-start.12 = (f32[1,256]{1,0:T(1,128)S(1)}, f32[1,256]{1,0:T(1,128)}, u32[]{:S(2)}) copy-start(f32[1,256]{1,0:T(1,128)} %slice.350) | copy-start | bytes 3076
  163.6 4.3 %copy-start.4 = (f32[255,256]{1,0:T(8,128)S(1)}, f32[255,256]{1,0:T(8,128)}, u32[]{:S(2)}) copy-start(f32[255,256]{1,0:T(8,128)} %slice.269) | copy-start | bytes 783364
  164.4 3.5 %slice-start = ((f32[512,256]{1,0:T(8,128)}), f32[1,256]{1,0:T(1,128)S(1)}, s32[]{:S(2)}) async-start(f32[512,256]{1,0:T(8,128)} %copy-done.2), calls=%async_computation.11 | async-start | bytes 2048 | tf_op jit(solution)/shard_map/slice | solution.py:152
  210.9 5.3 %copy-start.16 = (bf16[256]{0:T(256)(128)(2,1)S(1)}, bf16[256]{0:T(256)(128)(2,1)}, u32[]{:S(2)}) copy-start(bf16[256]{0:T(256)(128)(2,1)} %param.26) | copy-start | bytes 1540
  210.9 10.1 %copy-start.1 = (bf16[512,256]{1,0:T(8,128)(2,1)S(1)}, bf16[512,256]{1,0:T(8,128)(2,1)}, u32[]{:S(2)}) copy-start(bf16[512,256]{1,0:T(8,128)(2,1)} %param.17) | copy-start | bytes 786436
  210.9 14.9 %copy-start.17 = (bf16[256]{0:T(256)(128)(2,1)S(1)}, bf16[256]{0:T(256)(128)(2,1)}, u32[]{:S(2)}) copy-start(bf16[256]{0:T(256)(128)(2,1)} %param.27) | copy-start | bytes 1540
  212.0 9.0 %all-to-all-start.3 = ((f32[8,1,512]{2,1,0:T(1,128)}), f32[8,1,512]{2,1,0:T(1,128)S(1)}, u32[]{:S(2)}, u32[]{:S(2)}) async-start(f32[8,1,512]{2,1,0:T(1,128)} %broadcast_in_dim.14), calls=%async_computation.3 | async-start | bytes 32768 | tf_op jit(solution)/shard_map/all_to_all | solution.py:17
  221.9 8.5 %all-to-all-start.4 = ((f32[8,1,512]{2,1,0:T(1,128)}), f32[8,1,512]{2,1,0:T(1,128)S(1)}, u32[]{:S(2)}, u32[]{:S(2)}) async-start(f32[8,1,512]{2,1,0:T(1,128)} %broadcast_in_dim.15), calls=%async_computation.4 | async-start | bytes 32768 | tf_op jit(solution)/shard_map/all_to_all | solution.py:17
  232.3 4.4 %copy-start.10 = (bf16[3,704]{1,0:T(4,128)(2,1)S(1)}, bf16[3,704]{1,0:T(4,128)(2,1)}, u32[]{:S(2)}) copy-start(bf16[3,704]{1,0:T(4,128)(2,1)} %param.30) | copy-start | bytes 12676
  232.3 4.4 %copy-start.11 = (bf16[3,704]{1,0:T(4,128)(2,1)S(1)}, bf16[3,704]{1,0:T(4,128)(2,1)}, u32[]{:S(2)}) copy-start(bf16[3,704]{1,0:T(4,128)(2,1)} %param.31) | copy-start | bytes 12676
  232.3 30.6 %all-to-all-start.5 = ((bf16[8,512,256]{1,2,0:T(8,128)(2,1)}), bf16[8,512,256]{1,2,0:T(8,128)(2,1)S(1)}, u32[]{:S(2)}, u32[]{:S(2)}) async-start(bf16[8,512,256]{1,2,0:T(8,128)(2,1)} %broadcast_in_dim.16), calls=%async_computation.5 | async-start | bytes 4194304 | tf_op jit(solution)/shard_map/all_to_all | solution.py:17
  262.9 4.5 %copy-start.14 = (bf16[2048,2112]{1,0:T(8,128)(2,1)S(1)}, bf16[2048,2112]{1,0:T(8,128)(2,1)}, u32[]{:S(2)}) copy-start(bf16[2048,2112]{1,0:T(8,128)(2,1)} %all-gather.8.cloned.1.call-done) | copy-start | bytes 25952260
  304.1 5.4 %copy-start.18 = (bf16[256]{0:T(256)(128)(2,1)S(1)}, bf16[256]{0:T(256)(128)(2,1)}, u32[]{:S(2)}) copy-start(bf16[256]{0:T(256)(128)(2,1)} %param.33) | copy-start | bytes 1540
  305.2 9.0 %all-to-all-start.7 = ((f32[8,1,512]{2,1,0:T(1,128)}), f32[8,1,512]{2,1,0:T(1,128)S(1)}, u32[]{:S(2)}, u32[]{:S(2)}) async-start(f32[8,1,512]{2,1,0:T(1,128)} %broadcast_in_dim.17), calls=%async_computation.7 | async-start | bytes 32768 | tf_op jit(solution)/shard_map/all_to_all | solution.py:17
Sparse Core Ops, SparseCore 0:
  9.9 77.0 all-gather.3
  88.8 35.2 all-gather.5
  126.7 103.1 all-gather.7
where the time goes:
time: 325 us; the launch traced here: 322 us
  waiting for transfers between devices  88 us (27%)
  blocking collectives  77.2 us (24%)
  local copies, waits for them, and re-layouts  69.4 us (21%)
  starting transfers between devices  28.8 us (9%)
  other arithmetic  25.5 us (8%)
  matrix products  19 us (6%)
  between operations  13.6 us (4%)
    all_to_all x6, waiting for transfers between devices, sent_to_all(): lax.all_to_all(jnp.broadcast_to(shard[None], (devices, *shard.shape)), ax...  70.5 us
    all_to_all x2, blocking collectives, sent_and_summed(): lax.all_to_all(split_up(shard, dim, devices), axis, 0, 0, tiled=True)  65.2 us
    slice x54, local copies, waits for them, and re-layouts, shards(): _, states = lax.associative_scan(linear_combine, (retain, driven), axis=0)  55.8 us
    all_to_all x6, starting transfers between devices, sent_to_all(): lax.all_to_all(jnp.broadcast_to(shard[None], (devices, *shard.shape)), ax...  28.7 us
    all_gather x1, waiting for transfers between devices, in_one_piece(): lax.all_gather(both, axis, axis=dim, tiled=True)  17.5 us
    all_gather x1, blocking collectives, gather_axes(): shard = lax.all_gather(shard, axis, axis=dim, tiled=True)  12 us
    mul x7, other arithmetic, linear_combine(): return (earlier[0] * latter[0], latter[0] * earlier[1] + latter[1])  9.35 us
  transfers between devices with their start and end apart: 9, of which 7 were waited for; matrix products, arithmetic and copies ran while one was open for 31% of the time, Pallas kernels for 0%

commit v1 on v0

v1 whole, which is shorter than its diff:
```python
import functools
import jax
import jax.numpy as jnp
from jax import lax
from jax.experimental import pallas as pl
from jax.experimental.pallas import tpu as pltpu
from jax.sharding import Mesh
from jax.sharding import PartitionSpec as P

D = 2048
FS = ("z", "x")
TP = ("y", "c")
NZ, NX, NTP = 8, 4, 8
ROWS = 512
OWN = ROWS // NTP
PIECE = D // NTP
norm_eps = 1e-06
gate_power = 8.0
bf16, f32 = jnp.bfloat16, jnp.float32


def sent_to_all(shard, axis, devices):
    return lax.all_to_all(
        jnp.broadcast_to(shard[None], (devices, *shard.shape)), axis, 0, 0, tiled=True
    )


def row_normed(values, row_gain):
    widened = values.astype(f32)
    factor = lax.rsqrt(jnp.sum(widened * widened, axis=1, keepdims=True) / D + norm_eps)
    return widened * factor * row_gain.astype(f32)


def gelu(v):
    return 0.5 * v * (1.0 + jnp.tanh(0.7978845608028654 * (v + 0.044715 * v * v * v)))


def one_less_exp(u):
    s = 1.0 + u * (1.0 / 8.0)
    for k in range(7, 1, -1):
        s = 1.0 + u * (1.0 / k) * s
    return jnp.where(u > -0.5, -u * s, 1.0 - jnp.exp(u))


def shifted_down(values, by, rows):
    return jnp.where(rows >= by, pltpu.roll(values, by, 0), 0.0)


def mixer_kernel(
    x_ref, w_ref, taps_ref, recur_ref, inject_ref, slope_ref, o_ref,
    win_ref, wout_ref, keep_ref, drive_ref,
):
    for z in range(NZ):
        for x in range(NX):
            at = (z * NX + x) * 64
            win_ref[at : at + 64, :] = w_ref[x, z, :, 0:512]
            wout_ref[at : at + 64, :] = w_ref[x, z, :, 512:768]
    squares = jnp.zeros((ROWS, 1), f32)
    for k in range(NTP):
        v = x_ref[k, 0:ROWS, :].astype(f32)
        squares = squares + jnp.sum(v * v, axis=1, keepdims=True)
    factor = lax.rsqrt(squares / D + norm_eps)
    both = jnp.zeros((ROWS, 2 * PIECE), f32)
    for k in range(NTP):
        gain = x_ref[k, ROWS : ROWS + 1, :].astype(f32)
        v = (x_ref[k, 0:ROWS, :].astype(f32) * factor * gain).astype(bf16)
        both = both + jnp.dot(
            v, win_ref[k * PIECE : (k + 1) * PIECE, :], preferred_element_type=f32
        )
    gate_rows = both[:, 0:PIECE].astype(bf16)
    input_rows = both[:, PIECE:].astype(bf16).astype(f32)
    rows = lax.broadcasted_iota(jnp.int32, (ROWS, PIECE), 0)
    taps = taps_ref[...].astype(f32)
    smoothed = input_rows * taps[3:4, :]
    for back in (1, 2, 3):
        smoothed = smoothed + shifted_down(input_rows, back, rows) * taps[3 - back : 4 - back, :]
    smoothed = smoothed.astype(bf16)
    recur = jax.nn.sigmoid(jnp.dot(smoothed, recur_ref[...], preferred_element_type=f32))
    inject = jax.nn.sigmoid(jnp.dot(smoothed, inject_ref[...], preferred_element_type=f32))
    log_retain = -gate_power * recur * slope_ref[...]
    keep = jnp.exp(log_retain)
    drive = jnp.sqrt(one_less_exp(2.0 * log_retain)) * inject * smoothed.astype(f32)
    within = rows % 8
    for by in (1, 2, 4):
        ok = within >= by
        drive = jnp.where(ok, keep * pltpu.roll(drive, by, 0), 0.0) + drive
        keep = jnp.where(ok, pltpu.roll(keep, by, 0), 1.0) * keep
    keep_ref[...] = keep
    drive_ref[...] = drive

    def tile(i, carry):
        at = pl.ds(pl.multiple_of(i * 8, 8), 8)
        state = keep_ref[at, :] * carry + drive_ref[at, :]
        drive_ref[at, :] = state
        return state[7:8, :]

    lax.fori_loop(0, ROWS // 8, tile, jnp.zeros((1, PIECE), f32), unroll=8)
    hidden = (gelu(gate_rows.astype(f32)) * drive_ref[...]).astype(bf16)
    for k in range(NTP):
        o_ref[:, k * PIECE : (k + 1) * PIECE] = lax.dot_general(
            hidden, wout_ref[k * PIECE : (k + 1) * PIECE, :], (((1,), (1,)), ((), ())),
            preferred_element_type=f32,
        ).astype(bf16)


def mixer(x_all, w_all, taps, w_recur, w_inject, slope):
    vmem = pl.BlockSpec(memory_space=pltpu.VMEM)
    return pl.pallas_call(
        mixer_kernel,
        out_shape=jax.ShapeDtypeStruct((ROWS, D), bf16),
        in_specs=[vmem] * 6,
        out_specs=vmem,
        scratch_shapes=[
            pltpu.VMEM((D, 512), bf16),
            pltpu.VMEM((D, PIECE), bf16),
            pltpu.VMEM((ROWS, PIECE), f32),
            pltpu.VMEM((ROWS, PIECE), f32),
        ],
        compiler_params=pltpu.CompilerParams(vmem_limit_bytes=40 * 1024 * 1024),
        cost_estimate=pl.CostEstimate(
            flops=2 * ROWS * D * 768 + 4 * ROWS * PIECE * PIECE,
            bytes_accessed=8 * 1024 * 1024, transcendentals=ROWS * PIECE * 6,
        ),
        name="mixer",
    )(x_all, w_all, taps, w_recur, w_inject, slope)


def causal_conv(values, kernel):
    length = values.shape[0]
    widths = kernel.shape[0]
    padded = jnp.pad(values.astype(f32), ((widths - 1, 0), (0, 0)))
    weights = kernel.astype(f32)
    result = padded[0:length] * weights[0]
    for offset in range(1, widths):
        result = result + padded[offset : offset + length] * weights[offset]
    return result


def summed(pieces):
    return jnp.sum(pieces.astype(f32), axis=0)


def shards(
    tokens, pre_mix_gain, w_gate_in, w_input, mix_kernel, w_recur, w_inject, decay_param,
    w_mix_out, post_mix_gain, pre_ffn_gain, w_up_gate, w_up_value, gate_kernel, value_kernel,
    w_down, post_ffn_gain,
):
    ffn_own = jnp.concatenate([w_up_gate, w_up_value, w_down.T], axis=1)
    ffn_all = lax.all_gather(ffn_own, FS, axis=0, tiled=True)
    up_gate_all, up_value_all, down_all = jnp.split(ffn_all, [704, 1408], axis=1)

    gains = jnp.stack([pre_mix_gain, post_mix_gain, pre_ffn_gain, post_ffn_gain])
    packed = jnp.concatenate([tokens, jnp.pad(gains, ((0, 12), (0, 0)))], axis=0)
    mix_own = jnp.concatenate([w_gate_in, w_input, w_mix_out.T], axis=1)
    mix_z = sent_to_all(mix_own, "z", NZ)
    x_all = sent_to_all(packed, TP, NTP)
    mix_all = sent_to_all(mix_z.reshape(NZ, 64, 768), "x", NX).reshape(NX, NZ, 64, 768)
    x_all = x_all.reshape(NTP, ROWS + 16, PIECE)
    slope = jax.nn.softplus(-decay_param)[None, :]
    partial_mix = mixer(x_all, mix_all, mix_kernel, w_recur[0], w_inject[0], slope)

    me = lax.axis_index("y") * 2 + lax.axis_index("c")
    own_rows = lax.dynamic_slice(x_all, (0, me * OWN, 0), (NTP, OWN, PIECE))
    own_rows = own_rows.transpose(1, 0, 2).reshape(OWN, D)
    full_gains = x_all[:, ROWS : ROWS + 4, :].transpose(1, 0, 2).reshape(4, D)

    mixer_sum = summed(lax.all_to_all(partial_mix.reshape(NTP, OWN, D), TP, 0, 0, tiled=True))
    middle = (own_rows.astype(f32) + row_normed(mixer_sum, full_gains[1:2])).astype(bf16)
    normed_own = row_normed(middle, full_gains[2:3]).astype(bf16)
    normed_mid = sent_to_all(normed_own, TP, NTP).reshape(ROWS, D)

    up_gate = jnp.dot(normed_mid, up_gate_all, preferred_element_type=f32).astype(bf16)
    up_value = jnp.dot(normed_mid, up_value_all, preferred_element_type=f32).astype(bf16)
    conv_g = causal_conv(up_gate, gate_kernel)
    conv_v = causal_conv(up_value, value_kernel)
    activated = (jax.nn.gelu(conv_g, approximate=True) * conv_v).astype(bf16)
    partial_ffn = lax.dot_general(
        activated, down_all, (((1,), (1,)), ((), ())), preferred_element_type=f32
    ).astype(bf16)
    ffn_sum = summed(lax.all_to_all(partial_ffn.reshape(NTP, OWN, D), TP, 0, 0, tiled=True))
    out_rows = (middle.astype(f32) + row_normed(ffn_sum, full_gains[3:4])).astype(bf16)
    to_columns = out_rows.reshape(OWN, NTP, PIECE).transpose(1, 0, 2)
    return lax.all_to_all(to_columns, TP, 0, 0, tiled=True).reshape(ROWS, PIECE)


def solution(mesh):
    finer = Mesh(mesh.devices.reshape(NZ, NX, 4, 2), ("z", "x", "y", "c"))
    return jax.shard_map(
        shards,
        mesh=finer,
        in_specs=(
            P(FS, TP), P(TP), P(FS, TP), P(FS, TP), P(None, TP), P(TP, None, None),
            P(TP, None, None), P(TP), P(TP, FS), P(TP), P(TP), P(FS, TP), P(FS, TP),
            P(None, TP), P(None, TP), P(TP, FS), P(TP),
        ),
        out_specs=P(FS, TP),
        check_vma=False,
    )
```

time: 325 us -> 276 us (0.85)
  waiting for transfers between devices: 88 us -> 159 us
  local copies, waits for them, and re-layouts: 69.4 us -> 12 us
  blocking collectives: 77.2 us -> 42.5 us
  other arithmetic: 25.5 us -> 4.54 us
  matrix products: 19 us -> 12 us
  Pallas kernels: 0 us -> 4.42 us
    slice x54 -> x0, local copies, waits for them, and re-layouts: 55.8 us -> none  [shards(): _, states = lax.associative_scan(linear_combine, (retain, driven), axis=0)]
    all_to_all x0 -> x2, waiting for transfers between devices: none -> 50.6 us  [the longest x1 26.2 us: shards(): lax.all_to_all(partial_ffn.reshape(NTP, OWN, D), TP, 0, 0, tiled=True)]
    all_to_all x6 -> x3, waiting for transfers between devices: 70.5 us -> 108 us  [sent_to_all(): lax.all_to_all(jnp.broadcast_to(shard[None], (devices, *shard.shape)), ax...]
    all_to_all x2, blocking collectives: 65.2 us -> 42.5 us  [the longest x1 32.7 us: sent_to_all(): lax.all_to_all(jnp.broadcast_to(shard[None], (devices, *shard.shape)), ax...]
    all_gather x3 -> x1, waiting for transfers between devices: 17.5 us -> 0.01 us  [shards(): ffn_all = lax.all_gather(ffn_own, FS, axis=0, tiled=True)]
    all_gather x1 -> x0, blocking collectives: 12 us -> none  [gather_axes(): shard = lax.all_gather(shard, axis, axis=dim, tiled=True)]
    all_to_all x6 -> x3, starting transfers between devices: 28.7 us -> 18 us  [sent_to_all(): lax.all_to_all(jnp.broadcast_to(shard[None], (devices, *shard.shape)), ax...]
    all_to_all x0 -> x2, starting transfers between devices: none -> 9.59 us  [the longest x1 5.13 us: shards(): lax.all_to_all(partial_mix.reshape(NTP, OWN, D), TP, 0, 0, tiled=True)]
  transfers between devices with their start and end apart: 9 -> 6, of which waited for: 7 -> 5; matrix products, arithmetic and copies ran while one was open for 31% -> 3% of each run, Pallas kernels for 0% -> 2%
where the time goes in v1:
time: 276 us
  waiting for transfers between devices  159 us (58%)
  blocking collectives  42.5 us (15%)
  starting transfers between devices  27.6 us (10%)
  between operations  13.6 us (5%)
  local copies, waits for them, and re-layouts  12 us (4%)
  matrix products  12 us (4%)
  other arithmetic  4.54 us (2%)
  Pallas kernels  4.42 us (2%)
    all_to_all x3, waiting for transfers between devices, sent_to_all(): lax.all_to_all(jnp.broadcast_to(shard[None], (devices, *shard.shape)), ax...  108 us
    all_to_all x1, blocking collectives, sent_to_all(): lax.all_to_all(jnp.broadcast_to(shard[None], (devices, *shard.shape)), ax...  32.7 us
    all_to_all x1, waiting for transfers between devices, shards(): lax.all_to_all(partial_ffn.reshape(NTP, OWN, D), TP, 0, 0, tiled=True)  26.2 us
    all_to_all x1, waiting for transfers between devices, shards(): lax.all_to_all(partial_mix.reshape(NTP, OWN, D), TP, 0, 0, tiled=True)  24.4 us
    all_to_all x3, starting transfers between devices, sent_to_all(): lax.all_to_all(jnp.broadcast_to(shard[None], (devices, *shard.shape)), ax...  18 us
    all_to_all x1, blocking collectives, shards(): return lax.all_to_all(to_columns, TP, 0, 0, tiled=True).reshape(ROWS, PIECE)  9.84 us
  transfers between devices with their start and end apart: 6, of which 5 were waited for; matrix products, arithmetic and copies ran while one was open for 3% of the time, Pallas kernels for 2%

profile of v1, /device:TPU:1, one launch (start us, length us, event | category | flops | bytes accessed | tf_op | source)
XLA Modules:
  0.0 275.6 jit_solution(1427377780658182964)
XLA Ops:
  6.5 1.8 concatenate.11
  8.4 0.9 pad_maximum_fusion.1
  9.3 1.0 broadcast_in_dim.11
  10.3 9.0 %all-to-all-start.1 = ((bf16[8,64,768]{2,1,0:T(8,128)(2,1)}), bf16[8,64,768]{2,1,0:T(8,128)(2,1)S(1)}, u32[]{:S(2)}, u32[]{:S(2)}) async-start(bf16[8,64,768]{2,1,0:T(8,128)(2,1)} %broadcast_in_dim.11), calls=%async_computation.1 | async-start | bytes 1572864 | tf_op jit(solution)/shard_map/all_to_all | solution.py:23
  19.4 27.7 %all-to-all-done.1 = bf16[8,64,768]{2,1,0:T(8,128)(2,1)S(1)} async-done(((bf16[8,64,768]{2,1,0:T(8,128)(2,1)}), bf16[8,64,768]{2,1,0:T(8,128)(2,1)S(1)}, u32[]{:S(2)}, u32[]{:S(2)}) %all-to-all-start.1) | async-done | bytes 786464 | tf_op jit(solution)/shard_map/all_to_all | solution.py:23
  47.2 32.7 %all_to_all.35.x_ref = bf16[8,528,256]{2,1,0:T(8,128)(2,1)} all-to-all(bf16[8,528,256]{2,1,0:T(8,128)(2,1)S(1)} %broadcast_in_dim.10), channel_id=1, replica_groups=mesh['z'=8,'x'=4,'y'=4,'c'=2] {'y','c'}, dimensions={0} | all-to-all | bytes 4325376 | tf_op jit(solution)/shard_map/all_to_all | solution.py:23
  79.9 2.0 broadcast_in_dim.12
  81.9 4.4 %all-to-all-start.2 = ((bf16[4,8,64,768]{3,2,1,0:T(8,128)(2,1)}), bf16[4,8,64,768]{3,2,1,0:T(8,128)(2,1)S(1)}, u32[]{:S(2)}, u32[]{:S(2)}) async-start(bf16[4,8,64,768]{3,2,1,0:T(8,128)(2,1)} %broadcast_in_dim.12), calls=%async_computation.2 | async-start | bytes 6291456 | tf_op jit(solution)/shard_map/all_to_all | solution.py:23
  86.4 54.4 %all-to-all-done.2.w_ref = bf16[4,8,64,768]{3,2,1,0:T(8,128)(2,1)S(1)} async-done(((bf16[4,8,64,768]{3,2,1,0:T(8,128)(2,1)}), bf16[4,8,64,768]{3,2,1,0:T(8,128)(2,1)S(1)}, u32[]{:S(2)}, u32[]{:S(2)}) %all-to-all-start.2) | async-done | bytes 3145760 | tf_op jit(solution)/shard_map/all_to_all | solution.py:23
  140.8 1.6 copy-done
  142.4 4.4 %mixer.1 = bf16[512,2048]{1,0:T(8,128)(2,1)S(1)} custom-call(bf16[8,528,256]{2,1,0:T(8,128)(2,1)S(1)} %copy-done, bf16[4,8,64,768]{3,2,1,0:T(8,128)(2,1)S(1)} %all-to-all-done.2.w_ref, bf16[4,256]{1,0:T(4,128)(2,1)S(1)} %copy-done.4, bf16[256,256]{1,0:T(8,128)(2,1)S(1)} %bitcast.51, bf16[256,256]{1,0:T(8,128)(2,1)S(1)} %bitcast.52, f32[1,256]{1,0:T(1,128)S(1)} %bitcast.53), custom_call_target="tpu_custom_call" | custom-call | flops 1744830464 | bytes 8388608 | tf_op jit(solution)/shard_map/mixer/pallas_call | solution.py:108
  146.8 1.4 copy-done.1
  148.2 5.1 %all-to-all-start.3 = ((bf16[8,64,2048]{2,1,0:T(8,128)(2,1)}), bf16[8,64,2048]{2,1,0:T(8,128)(2,1)S(1)}, u32[]{:S(2)}, u32[]{:S(2)}) async-start(bf16[8,64,2048]{2,1,0:T(8,128)(2,1)} %bitcast.50), calls=%async_computation.3 | async-start | bytes 4194304 | tf_op jit(solution)/shard_map/all_to_all | solution.py:167
  153.3 0.8 slice_bitcast_fusion
  154.1 1.0 convert_bitcast_fusion
  155.2 24.4 %all-to-all-done.3 = bf16[8,64,2048]{2,1,0:T(8,128)(2,1)S(1)} async-done(((bf16[8,64,2048]{2,1,0:T(8,128)(2,1)}), bf16[8,64,2048]{2,1,0:T(8,128)(2,1)S(1)}, u32[]{:S(2)}, u32[]{:S(2)}) %all-to-all-start.3) | async-done | bytes 2097184 | tf_op jit(solution)/shard_map/all_to_all | solution.py:167
  179.5 0.4 convert_reduce_fusion.1
  180.1 1.3 fusion.49
  181.3 0.2 multiply_convert_fusion
  181.5 1.6 broadcast_in_dim.14
  183.2 4.6 %all-to-all-start.4 = ((bf16[8,64,2048]{2,1,0:T(8,128)(2,1)}), bf16[8,64,2048]{2,1,0:T(8,128)(2,1)S(1)}, u32[]{:S(2)}, u32[]{:S(2)}) async-start(bf16[8,64,2048]{2,1,0:T(8,128)(2,1)} %broadcast_in_dim.14), calls=%async_computation.4 | async-start | bytes 4194304 | tf_op jit(solution)/shard_map/all_to_all | solution.py:23
  187.9 26.1 %all-to-all-done.4 = bf16[8,64,2048]{2,1,0:T(8,128)(2,1)S(1)} async-done(((bf16[8,64,2048]{2,1,0:T(8,128)(2,1)}), bf16[8,64,2048]{2,1,0:T(8,128)(2,1)S(1)}, u32[]{:S(2)}, u32[]{:S(2)}) %all-to-all-start.4) | async-done | bytes 2097184 | tf_op jit(solution)/shard_map/all_to_all | solution.py:23
  214.0 3.7 %fusion.29 = f32[512,704]{0,1:T(8,128)S(1)} fusion(bf16[512,2048]{1,0:T(8,128)(2,1)S(1)} %bitcast.56, bf16[2048,2112]{1,0:T(8,128)(2,1)} %all-gather.2.cloned.1.call-done), kind=kOutput, calls=%fused_computation.32 | convolution fusion | flops 1477115904 | bytes 6684672 | tf_op jit(solution)/shard_map/dot_general | solution.py:172
  217.7 0.7 copy-done.9
  218.5 2.9 %fusion.35 = f32[512,704]{0,1:T(8,128)S(1)} fusion(bf16[512,2048]{1,0:T(8,128)(2,1)S(1)} %bitcast.57, bf16[2048,2112]{1,0:T(8,128)(2,1)S(1)} %copy-done.9), kind=kOutput, calls=%fused_computation.34 | convolution fusion | flops 1477115904 | bytes 6684672 | tf_op jit(solution)/shard_map/dot_general | solution.py:173
  221.4 5.4 %fusion.6 = bf16[512,2048]{1,0:T(8,128)(2,1)} fusion(bf16[2048,2112]{1,0:T(8,128)(2,1)S(1)} %copy-done.9, f32[512,704]{0,1:T(8,128)S(1)} %fusion.35, f32[512,704]{0,1:T(8,128)S(1)} %fusion.29, f32[704]{0:T(1024)S(1)} %get-tuple-element.9, f32[704]{0:T(1024)S(1)} %get-tuple-element.10, f32[704]{0:T(1024)S(1)} %get-tuple-element.8, ...), kind=kOutput, calls=%fused_computation.8 | convolution fusion | flops 1484652544 | bytes 8151040 | tf_op jit(solution)/shard_map/dot_general | solution.py:177
  226.8 4.5 %all-to-all-start.5 = ((bf16[8,64,2048]{2,1,0:T(8,128)(2,1)}), bf16[8,64,2048]{2,1,0:T(8,128)(2,1)S(1)}, u32[]{:S(2)}, u32[]{:S(2)}) async-start(bf16[8,64,2048]{2,1,0:T(8,128)(2,1)} %bitcast.58), calls=%async_computation.5 | async-start | bytes 4194304 | tf_op jit(solution)/shard_map/all_to_all | solution.py:180
  231.3 26.2 %all-to-all-done.5 = bf16[8,64,2048]{2,1,0:T(8,128)(2,1)S(1)} async-done(((bf16[8,64,2048]{2,1,0:T(8,128)(2,1)}), bf16[8,64,2048]{2,1,0:T(8,128)(2,1)S(1)}, u32[]{:S(2)}, u32[]{:S(2)}) %all-to-all-start.5) | async-done | bytes 2097184 | tf_op jit(solution)/shard_map/all_to_all | solution.py:180
  257.5 0.3 convert_reduce_fusion
  258.0 0.2 fusion.55
  258.2 9.8 %all_to_all.36 = bf16[8,64,256]{2,1,0:T(8,128)(2,1)S(1)} all-to-all(bf16[8,64,256]{2,1,0:T(8,128)(2,1)S(1)} %fusion.55), channel_id=1, replica_groups=mesh['z'=8,'x'=4,'y'=4,'c'=2] {'y','c'}, dimensions={0} | all-to-all | bytes 524288 | tf_op jit(solution)/shard_map/all_to_all | solution.py:183
  268.0 0.7 copy.36
  (48 shorter events, 0.7 us)
Async XLA Ops:
  6.5 207.5 %all-gather.2.cloned.1.call-start = ((), (), s32[]{:S(2)}) async-start(), calls=%async_computation.7 | async-start | bytes 9191424 | tf_op jit(solution)/shard_map/all_gather | solution.py:149
  8.4 10.9 %copy-start.10 = (bf16[256]{0:T(256)(128)(2,1)S(1)}, bf16[256]{0:T(256)(128)(2,1)}, u32[]{:S(2)}) copy-start(bf16[256]{0:T(256)(128)(2,1)} %param.18) | copy-start | bytes 1540
  8.4 11.0 %copy-start.11 = (bf16[256]{0:T(256)(128)(2,1)S(1)}, bf16[256]{0:T(256)(128)(2,1)}, u32[]{:S(2)}) copy-start(bf16[256]{0:T(256)(128)(2,1)} %param.26) | copy-start | bytes 1540
  8.4 11.0 %copy-start.12 = (bf16[256]{0:T(256)(128)(2,1)S(1)}, bf16[256]{0:T(256)(128)(2,1)}, u32[]{:S(2)}) copy-start(bf16[256]{0:T(256)(128)(2,1)} %param.27) | copy-start | bytes 1540
  8.4 11.0 %copy-start.13 = (bf16[256]{0:T(256)(128)(2,1)S(1)}, bf16[256]{0:T(256)(128)(2,1)}, u32[]{:S(2)}) copy-start(bf16[256]{0:T(256)(128)(2,1)} %param.33) | copy-start | bytes 1540
  8.4 11.0 %copy-start.5 = (bf16[512,256]{1,0:T(8,128)(2,1)S(1)}, bf16[512,256]{1,0:T(8,128)(2,1)}, u32[]{:S(2)}) copy-start(bf16[512,256]{1,0:T(8,128)(2,1)} %param.17) | copy-start | bytes 786436
  10.3 36.8 %all-to-all-start.1 = ((bf16[8,64,768]{2,1,0:T(8,128)(2,1)}), bf16[8,64,768]{2,1,0:T(8,128)(2,1)S(1)}, u32[]{:S(2)}, u32[]{:S(2)}) async-start(bf16[8,64,768]{2,1,0:T(8,128)(2,1)} %broadcast_in_dim.11), calls=%async_computation.1 | async-start | bytes 1572864 | tf_op jit(solution)/shard_map/all_to_all | solution.py:23
  81.9 4.4 %copy-start.8 = (f32[256]{0:T(256)S(1)}, f32[256]{0:T(256)}, u32[]{:S(2)}) copy-start(f32[256]{0:T(256)} %param.24) | copy-start | bytes 3076
  81.9 58.9 %copy-start.2 = (bf16[1,256,256]{2,1,0:T(8,128)(2,1)S(1)}, bf16[1,256,256]{2,1,0:T(8,128)(2,1)}, u32[]{:S(2)}) copy-start(bf16[1,256,256]{2,1,0:T(8,128)(2,1)} %param.22) | copy-start | bytes 393220
  81.9 58.9 %copy-start.3 = (bf16[1,256,256]{2,1,0:T(8,128)(2,1)S(1)}, bf16[1,256,256]{2,1,0:T(8,128)(2,1)}, u32[]{:S(2)}) copy-start(bf16[1,256,256]{2,1,0:T(8,128)(2,1)} %param.23) | copy-start | bytes 393220
  81.9 58.9 %copy-start.4 = (bf16[4,256]{1,0:T(4,128)(2,1)S(1)}, bf16[4,256]{1,0:T(4,128)(2,1)}, u32[]{:S(2)}) copy-start(bf16[4,256]{1,0:T(4,128)(2,1)} %taps_ref.1) | copy-start | bytes 6148
  81.9 58.8 %all-to-all-start.2 = ((bf16[4,8,64,768]{3,2,1,0:T(8,128)(2,1)}), bf16[4,8,64,768]{3,2,1,0:T(8,128)(2,1)S(1)}, u32[]{:S(2)}, u32[]{:S(2)}) async-start(bf16[4,8,64,768]{3,2,1,0:T(8,128)(2,1)} %broadcast_in_dim.12), calls=%async_computation.2 | async-start | bytes 6291456 | tf_op jit(solution)/shard_map/all_to_all | solution.py:23
  140.8 1.6 copy-start
  146.8 1.4 copy-start.1
  148.2 31.3 %all-to-all-start.3 = ((bf16[8,64,2048]{2,1,0:T(8,128)(2,1)}), bf16[8,64,2048]{2,1,0:T(8,128)(2,1)S(1)}, u32[]{:S(2)}, u32[]{:S(2)}) async-start(bf16[8,64,2048]{2,1,0:T(8,128)(2,1)} %bitcast.50), calls=%async_computation.3 | async-start | bytes 4194304 | tf_op jit(solution)/shard_map/all_to_all | solution.py:167
  183.2 4.6 %copy-start.6 = (bf16[3,704]{1,0:T(4,128)(2,1)S(1)}, bf16[3,704]{1,0:T(4,128)(2,1)}, u32[]{:S(2)}) copy-start(bf16[3,704]{1,0:T(4,128)(2,1)} %param.30) | copy-start | bytes 12676
  183.2 4.6 %copy-start.7 = (bf16[3,704]{1,0:T(4,128)(2,1)S(1)}, bf16[3,704]{1,0:T(4,128)(2,1)}, u32[]{:S(2)}) copy-start(bf16[3,704]{1,0:T(4,128)(2,1)} %param.31) | copy-start | bytes 12676
  183.2 30.8 %all-to-all-start.4 = ((bf16[8,64,2048]{2,1,0:T(8,128)(2,1)}), bf16[8,64,2048]{2,1,0:T(8,128)(2,1)S(1)}, u32[]{:S(2)}, u32[]{:S(2)}) async-start(bf16[8,64,2048]{2,1,0:T(8,128)(2,1)} %broadcast_in_dim.14), calls=%async_computation.4 | async-start | bytes 4194304 | tf_op jit(solution)/shard_map/all_to_all | solution.py:23
  214.0 4.5 %copy-start.9 = (bf16[2048,2112]{1,0:T(8,128)(2,1)S(1)}, bf16[2048,2112]{1,0:T(8,128)(2,1)}, u32[]{:S(2)}) copy-start(bf16[2048,2112]{1,0:T(8,128)(2,1)} %all-gather.2.cloned.1.call-done) | copy-start | bytes 25952260
  226.8 30.7 %all-to-all-start.5 = ((bf16[8,64,2048]{2,1,0:T(8,128)(2,1)}), bf16[8,64,2048]{2,1,0:T(8,128)(2,1)S(1)}, u32[]{:S(2)}, u32[]{:S(2)}) async-start(bf16[8,64,2048]{2,1,0:T(8,128)(2,1)} %bitcast.58), calls=%async_computation.5 | async-start | bytes 4194304 | tf_op jit(solution)/shard_map/all_to_all | solution.py:180
Sparse Core Ops, SparseCore 0:
  9.9 128.5 all-gather.1
